TPU v7x, 512 devices: a whole 4x8x8 slice. The times are simulated.
512 devices in a mesh: ep: 32 (over z, x), tp: 16 (over y, core).
Axes of the slice: x: 4, y: 8, z: 8, core: 2. Of those that a mesh axis runs over, the one named last changes fastest.
Arguments:
- queries: bfloat16 [12288, 2048], P('ep', 'tp'), may hold values from -8 to 8
- keys: bfloat16 [12288, 2048], P('ep', 'tp'), may hold values from -8 to 8
- values: bfloat16 [12288, 2048], P('ep', 'tp'), may hold values from -6 to 6
- key_offset: bfloat16 [12288, 16], P('ep', 'tp'), may hold values from -15.25 to -0.4
- rows: bfloat16 [4096, 2048], P('ep'), may hold values from -6 to 6
- gain: float32 [2048], replicated, may hold values from 0.1 to 1.9
- gate_w: bfloat16 [32, 2048, 3584], P('ep', None, 'tp'), may hold values from -0.125 to 0.125
- up_w: bfloat16 [32, 2048, 3584], P('ep', None, 'tp'), may hold values from -0.125 to 0.125
- down_w: bfloat16 [32, 3584, 2048], P('ep', 'tp'), may hold values from -0.09375 to 0.09375
- expert_ids: int32 [4096, 2], P('ep'), may hold values from 0 to 31, all different within a row; in each aligned block of 128 rows (0 to 127, 128 to 255, ...) at most 16 rows name the same one
- route_weights: float32 [4096, 2], P('ep'), may hold values from 0.2 to 1
Outputs:
- attended: bfloat16 [12288, 2048], P('ep', 'tp')
- mixed: bfloat16 [4096, 2048], P('ep')
Inputs may be any that keep to these rules, and one draw needn't show every extreme that they name: `expert_ids`: each token names 2 different experts; among the 128 tokens of one ep index no expert is chosen more than 16 times, and in some such block an expert is chosen exactly 16 times.
All inputs are finite; a program needn't handle non-finite values.
Results may differ from a plain program's by a relative error of at most 0.019.
Values may be sent and summed in bfloat16 or wider, within the bound.
No kernel may reach another device: no remote copies, remote signals or barrier semaphores. Data moves between devices by JAX's collectives and lax.ppermute only.
A program may use at most 128 MiB of HBM per device.

v0:
```python
import jax
import jax.numpy as jnp
from jax import lax
from jax.sharding import PartitionSpec as P

EPSILON = 1e-06


def in_blocks(x, dim, peers):
    before, after = (x.shape[:dim], x.shape[dim + 1 :])
    return jnp.moveaxis(x.reshape(*before, peers, -1, *after), dim, 0)


def sent_and_summed(x, axis, dim):
    parts = in_blocks(x, dim, lax.axis_size(axis))
    arrived = lax.all_to_all(parts, axis, split_axis=0, concat_axis=0, tiled=True)
    return arrived.astype(jnp.float32).sum(axis=0)


def joined_along(parts, dim):
    shape = list(parts.shape[1:])
    shape[dim] *= parts.shape[0]
    return jnp.moveaxis(parts, 0, dim).reshape(shape)


def sent_to_all(x, axis):
    copies = jnp.broadcast_to(x, (lax.axis_size(axis), *x.shape))
    return lax.all_to_all(copies, axis, split_axis=0, concat_axis=0, tiled=True)


def collect(x, axis, dim):
    return joined_along(sent_to_all(x, axis), dim)


def stick_mixer(queries, keys, values, key_offset):
    position = lax.axis_index("ep")
    query_len = queries.shape[0]
    heads = key_offset.shape[1]
    head_dim = queries.shape[1] // heads
    scale = head_dim ** (-0.5)
    query_heads = queries.reshape(query_len, heads, head_dim)
    query_pos = position * query_len + jnp.arange(query_len, dtype=jnp.int32)
    last_row = (position + 1) * query_len
    key_piece = lax.all_gather(keys, "ep", axis=0, tiled=True)
    value_piece = lax.all_gather(values, "ep", axis=0, tiled=True)
    offset_piece = lax.all_gather(key_offset, "ep", axis=0, tiled=True)
    block_count = key_piece.shape[0] // query_len
    key_split = key_piece.reshape(block_count, query_len, heads, head_dim)
    value_split = value_piece.reshape(block_count, query_len, heads, head_dim)
    offset_split = offset_piece.reshape(block_count, query_len, heads)

    def compute_block(key_here, value_here, offset_here, key_start):
        key_pos = key_start + jnp.arange(query_len, dtype=jnp.int32)
        logits = (
            jnp.einsum("qhd,khd->hqk", query_heads, key_here, preferred_element_type=jnp.float32)
            * scale
        )
        logits = logits + offset_here.astype(jnp.float32).T[:, None, :]
        strict = key_pos[None, None, :] < query_pos[None, :, None]
        breaks = jnp.where(strict, jax.nn.log_sigmoid(-logits), 0.0)
        within = lax.cumsum(breaks, axis=2, reverse=True) - breaks
        local = jnp.where(strict, jnp.exp(jax.nn.log_sigmoid(logits) + within), 0.0).astype(
            jnp.bfloat16
        )
        summed = jnp.einsum("hqk,khd->hqd", local, value_here, preferred_element_type=jnp.float32)
        return (summed, jnp.sum(breaks, axis=2))

    def skip_block(key_here, value_here, offset_here, key_start):
        return (
            jnp.zeros((heads, query_len, head_dim), jnp.float32),
            jnp.zeros((heads, query_len), jnp.float32),
        )

    def one_block(args):
        key_here, value_here, offset_here, block_index = args
        key_start = block_index * query_len
        return lax.cond(
            key_start < last_row,
            compute_block,
            skip_block,
            key_here,
            value_here,
            offset_here,
            key_start,
        )

    sums, totals = lax.map(
        one_block, (key_split, value_split, offset_split, jnp.arange(block_count, dtype=jnp.int32))
    )
    sums, totals = (sums, totals)
    later = lax.cumsum(totals, axis=0, reverse=True) - totals
    combined = jnp.einsum("bhq,bhqd->qhd", jnp.exp(later), sums)
    return combined.reshape(query_len, heads * head_dim).astype(jnp.bfloat16)


def routed_experts(rows, gain, gate_w, up_w, down_w, expert_ids, route_weights):
    ep_count = lax.axis_size("ep")
    local_experts = gate_w.shape[0]
    experts_all = ep_count * local_experts
    token_count = rows.shape[0]
    choose_count = expert_ids.shape[1]
    width = rows.shape[1]
    capacity = 2 * choose_count * token_count // experts_all
    rows_float = rows.astype(jnp.float32)
    normed = rows_float * lax.rsqrt(
        jnp.mean(rows_float * rows_float, axis=1, keepdims=True) + EPSILON
    )
    normed = (normed * gain[None, :]).astype(jnp.bfloat16)
    flat_ids = expert_ids.reshape(-1)
    onehot = (flat_ids[:, None] == jnp.arange(experts_all, dtype=jnp.int32)[None, :]).astype(
        jnp.int32
    )
    ranked = jnp.sum((jnp.cumsum(onehot, axis=0) - onehot) * onehot, axis=1)
    token_of = jnp.arange(token_count * choose_count, dtype=jnp.int32) // choose_count
    source_rows = (
        jnp.zeros((experts_all * capacity,), jnp.int32)
        .at[flat_ids * capacity + ranked]
        .set(token_of)
    )
    outgoing = normed[source_rows].reshape(ep_count, local_experts, capacity, width)
    arrived = lax.all_to_all(outgoing, "ep", split_axis=0, concat_axis=0, tiled=True)
    gate_val = jnp.einsum("sxcd,xdf->csxf", arrived, gate_w, preferred_element_type=jnp.float32)
    up_val = jnp.einsum("sxcd,xdf->csxf", arrived, up_w, preferred_element_type=jnp.float32)
    hidden = (jax.nn.silu(gate_val) * up_val).astype(jnp.bfloat16)
    share = sent_and_summed(
        jnp.einsum("csxf,xfd->csxd", hidden, down_w, preferred_element_type=jnp.float32).astype(
            jnp.bfloat16
        ),
        "tp",
        0,
    ).astype(jnp.bfloat16)
    returned = lax.all_to_all(share, "ep", split_axis=1, concat_axis=1, tiled=True)
    whole_slots = collect(returned, "tp", 0)
    flat_out = whole_slots.reshape(capacity * experts_all, width)
    slot_index = ranked * experts_all + flat_ids
    picked = flat_out[slot_index].astype(jnp.float32).reshape(token_count, choose_count, width)
    return jnp.sum(picked * route_weights[:, :, None], axis=1).astype(jnp.bfloat16)


def body(
    queries, keys, values, key_offset, rows, gain, gate_w, up_w, down_w, expert_ids, route_weights
):
    attended = stick_mixer(queries, keys, values, key_offset)
    mixed = routed_experts(rows, gain, gate_w, up_w, down_w, expert_ids, route_weights)
    return (attended, mixed)


def solution(mesh):
    in_specs = (
        P("ep", "tp"),
        P("ep", "tp"),
        P("ep", "tp"),
        P("ep", "tp"),
        P("ep", None),
        P(),
        P("ep", None, "tp"),
        P("ep", None, "tp"),
        P("ep", "tp", None),
        P("ep", None),
        P("ep", None),
    )
    out_specs = (P("ep", "tp"), P("ep", None))
    return jax.shard_map(body, mesh=mesh, in_specs=in_specs, out_specs=out_specs, check_vma=False)
```

profile of v0, /device:TPU:463, one launch (start us, length us, event | category | flops | bytes accessed | tf_op | source)
XLA Modules:
  0.0 519.0 jit_solution(13295193791613204802)
XLA Ops:
  24.6 48.0 %all-to-all-done = bf16[32,1,16,2048]{3,2,1,0:T(8,128)(2,1)S(1)} async-done(((bf16[32,1,16,2048]{3,2,1,0:T(8,128)(2,1)}), bf16[32,1,16,2048]{3,2,1,0:T(8,128)(2,1)S(1)}, u32[]{:S(2)}, u32[]{:S(2)}) %all-to-all-start) | async-done | bytes 2097184 | tf_op jit(solution)/shard_map/all_to_all | solution.py:121
  76.1 58.9 %all_to_all.23 = bf16[16,1,32,1,2048]{4,2,3,1,0:T(8,128)(2,1)S(1)} all-to-all(bf16[16,1,32,1,2048]{4,2,3,1,0:T(8,128)(2,1)S(1)} %fusion.22), channel_id=1, replica_groups=mesh['ep'=32,'tp'=16] {'tp'}, dimensions={0} | all-to-all | bytes 4194304 | tf_op jit(solution)/shard_map/all_to_all | solution.py:16
  138.3 9.8 %all-to-all-start.2 = ((bf16[32,2,1024]{2,1,0:T(2,128)(2,1)}), bf16[32,2,1024]{2,1,0:T(2,128)(2,1)S(1)}, u32[]{:S(2)}, u32[]{:S(2)}) async-start(bf16[32,2,1024]{2,1,0:T(2,128)(2,1)} %reshape.303), calls=%async_computation.2 | async-start | bytes 262144 | tf_op jit(solution)/shard_map/all_to_all | solution.py:132
  148.2 37.1 %all_gather.10 = bf16[12288,1]{0,1:T(2,128)(2,1)S(1)} all-gather(bf16[384,1]{0,1:T(2,128)(2,1)S(1)} %copy-done.1), channel_id=1, replica_groups=mesh['ep'=32,'tp'=16] {'ep'}, dimensions={0}, use_global_device_ids=true | all-gather | bytes 25344 | tf_op jit(solution)/shard_map/all_gather | solution.py:46
  187.4 16.1 %all-to-all-start.3 = ((bf16[16,1,32,1,2048]{4,2,3,1,0:T(8,128)(2,1)}), bf16[16,1,32,1,2048]{4,2,3,1,0:T(8,128)(2,1)}, u32[]{:S(2)}, u32[]{:S(2)}) async-start(bf16[16,1,32,1,2048]{4,2,3,1,0:T(8,128)(2,1)} %broadcast_in_dim.46), calls=%async_computation.3 | async-start | bytes 4194304 | tf_op jit(solution)/shard_map/all_to_all | solution.py:28
  203.7 291.9 %while.13 = (s32[]{:T(128)}, bf16[32,1,384,128]{3,2,1,0:T(8,128)(2,1)}, f32[32,1,384]{2,1,0:T(1,128)S(1)}, s32[32]{0:T(128)S(1)}, s32[]{:T(128)}, /*index=5*/bf1...) while((s32[]{:T(128)}, ...), condition=%wide.region_6.7_spmd.clone, body=%wide.region_0.6_spmd.clone.sunk | while | flops 99241728 | bytes 5957639 | solution.py:87
  204.9 7.2 %conditional.3 = (bf16[1,1,384,128]{3,2,1,0:T(8,128)(2,1)S(1)}, f32[1,1,384]{2,1,0:T(1,128)S(1)}) conditional(s32[]{:T(128)} %convert_element_type.99, () %tuple.52, (s32[]{:T(128)}, s32[]{:T(128)}, bf16[32,384,1,128]{3,1,2,0:T(8,128)(2,1)}, s32[]{:T(128)}, bf16[384,1,128]{2,0,1:T(8,128)(2,1)S(1)}, /*index=5*/bf16[32,384,1]{1,0,2:T(8,128)(2,1)S(1)}, ...), branch_computations={%region_1.1_spmd, %region_2.5_spmd} | conditional | flops 99241728 | bytes 5755680 | solution.py:77
  241.4 7.2 %conditional.3 = (bf16[1,1,384,128]{3,2,1,0:T(8,128)(2,1)S(1)}, f32[1,1,384]{2,1,0:T(1,128)S(1)}) conditional(s32[]{:T(128)} %convert_element_type.99, () %tuple.52, (s32[]{:T(128)}, s32[]{:T(128)}, bf16[32,384,1,128]{3,1,2,0:T(8,128)(2,1)}, s32[]{:T(128)}, bf16[384,1,128]{2,0,1:T(8,128)(2,1)S(1)}, /*index=5*/bf16[32,384,1]{1,0,2:T(8,128)(2,1)S(1)}, ...), branch_computations={%region_1.1_spmd, %region_2.5_spmd} | conditional | flops 99241728 | bytes 5755680 | solution.py:77
  268.8 7.2 %conditional.3 = (bf16[1,1,384,128]{3,2,1,0:T(8,128)(2,1)S(1)}, f32[1,1,384]{2,1,0:T(1,128)S(1)}) conditional(s32[]{:T(128)} %convert_element_type.99, () %tuple.52, (s32[]{:T(128)}, s32[]{:T(128)}, bf16[32,384,1,128]{3,1,2,0:T(8,128)(2,1)}, s32[]{:T(128)}, bf16[384,1,128]{2,0,1:T(8,128)(2,1)S(1)}, /*index=5*/bf16[32,384,1]{1,0,2:T(8,128)(2,1)S(1)}, ...), branch_computations={%region_1.1_spmd, %region_2.5_spmd} | conditional | flops 99241728 | bytes 5755680 | solution.py:77
  277.9 7.2 %conditional.3 = (bf16[1,1,384,128]{3,2,1,0:T(8,128)(2,1)S(1)}, f32[1,1,384]{2,1,0:T(1,128)S(1)}) conditional(s32[]{:T(128)} %convert_element_type.99, () %tuple.52, (s32[]{:T(128)}, s32[]{:T(128)}, bf16[32,384,1,128]{3,1,2,0:T(8,128)(2,1)}, s32[]{:T(128)}, bf16[384,1,128]{2,0,1:T(8,128)(2,1)S(1)}, /*index=5*/bf16[32,384,1]{1,0,2:T(8,128)(2,1)S(1)}, ...), branch_computations={%region_1.1_spmd, %region_2.5_spmd} | conditional | flops 99241728 | bytes 5755680 | solution.py:77
  287.0 7.2 %conditional.3 = (bf16[1,1,384,128]{3,2,1,0:T(8,128)(2,1)S(1)}, f32[1,1,384]{2,1,0:T(1,128)S(1)}) conditional(s32[]{:T(128)} %convert_element_type.99, () %tuple.52, (s32[]{:T(128)}, s32[]{:T(128)}, bf16[32,384,1,128]{3,1,2,0:T(8,128)(2,1)}, s32[]{:T(128)}, bf16[384,1,128]{2,0,1:T(8,128)(2,1)S(1)}, /*index=5*/bf16[32,384,1]{1,0,2:T(8,128)(2,1)S(1)}, ...), branch_computations={%region_1.1_spmd, %region_2.5_spmd} | conditional | flops 99241728 | bytes 5755680 | solution.py:77
  296.1 7.2 %conditional.3 = (bf16[1,1,384,128]{3,2,1,0:T(8,128)(2,1)S(1)}, f32[1,1,384]{2,1,0:T(1,128)S(1)}) conditional(s32[]{:T(128)} %convert_element_type.99, () %tuple.52, (s32[]{:T(128)}, s32[]{:T(128)}, bf16[32,384,1,128]{3,1,2,0:T(8,128)(2,1)}, s32[]{:T(128)}, bf16[384,1,128]{2,0,1:T(8,128)(2,1)S(1)}, /*index=5*/bf16[32,384,1]{1,0,2:T(8,128)(2,1)S(1)}, ...), branch_computations={%region_1.1_spmd, %region_2.5_spmd} | conditional | flops 99241728 | bytes 5755680 | solution.py:77
  305.3 7.2 %conditional.3 = (bf16[1,1,384,128]{3,2,1,0:T(8,128)(2,1)S(1)}, f32[1,1,384]{2,1,0:T(1,128)S(1)}) conditional(s32[]{:T(128)} %convert_element_type.99, () %tuple.52, (s32[]{:T(128)}, s32[]{:T(128)}, bf16[32,384,1,128]{3,1,2,0:T(8,128)(2,1)}, s32[]{:T(128)}, bf16[384,1,128]{2,0,1:T(8,128)(2,1)S(1)}, /*index=5*/bf16[32,384,1]{1,0,2:T(8,128)(2,1)S(1)}, ...), branch_computations={%region_1.1_spmd, %region_2.5_spmd} | conditional | flops 99241728 | bytes 5755680 | solution.py:77
  332.6 7.2 %conditional.3 = (bf16[1,1,384,128]{3,2,1,0:T(8,128)(2,1)S(1)}, f32[1,1,384]{2,1,0:T(1,128)S(1)}) conditional(s32[]{:T(128)} %convert_element_type.99, () %tuple.52, (s32[]{:T(128)}, s32[]{:T(128)}, bf16[32,384,1,128]{3,1,2,0:T(8,128)(2,1)}, s32[]{:T(128)}, bf16[384,1,128]{2,0,1:T(8,128)(2,1)S(1)}, /*index=5*/bf16[32,384,1]{1,0,2:T(8,128)(2,1)S(1)}, ...), branch_computations={%region_1.1_spmd, %region_2.5_spmd} | conditional | flops 99241728 | bytes 5755680 | solution.py:77
  350.9 7.2 %conditional.3 = (bf16[1,1,384,128]{3,2,1,0:T(8,128)(2,1)S(1)}, f32[1,1,384]{2,1,0:T(1,128)S(1)}) conditional(s32[]{:T(128)} %convert_element_type.99, () %tuple.52, (s32[]{:T(128)}, s32[]{:T(128)}, bf16[32,384,1,128]{3,1,2,0:T(8,128)(2,1)}, s32[]{:T(128)}, bf16[384,1,128]{2,0,1:T(8,128)(2,1)S(1)}, /*index=5*/bf16[32,384,1]{1,0,2:T(8,128)(2,1)S(1)}, ...), branch_computations={%region_1.1_spmd, %region_2.5_spmd} | conditional | flops 99241728 | bytes 5755680 | solution.py:77
  396.5 7.2 %conditional.3 = (bf16[1,1,384,128]{3,2,1,0:T(8,128)(2,1)S(1)}, f32[1,1,384]{2,1,0:T(1,128)S(1)}) conditional(s32[]{:T(128)} %convert_element_type.99, () %tuple.52, (s32[]{:T(128)}, s32[]{:T(128)}, bf16[32,384,1,128]{3,1,2,0:T(8,128)(2,1)}, s32[]{:T(128)}, bf16[384,1,128]{2,0,1:T(8,128)(2,1)S(1)}, /*index=5*/bf16[32,384,1]{1,0,2:T(8,128)(2,1)S(1)}, ...), branch_computations={%region_1.1_spmd, %region_2.5_spmd} | conditional | flops 99241728 | bytes 5755680 | solution.py:77
  405.6 7.2 %conditional.3 = (bf16[1,1,384,128]{3,2,1,0:T(8,128)(2,1)S(1)}, f32[1,1,384]{2,1,0:T(1,128)S(1)}) conditional(s32[]{:T(128)} %convert_element_type.99, () %tuple.52, (s32[]{:T(128)}, s32[]{:T(128)}, bf16[32,384,1,128]{3,1,2,0:T(8,128)(2,1)}, s32[]{:T(128)}, bf16[384,1,128]{2,0,1:T(8,128)(2,1)S(1)}, /*index=5*/bf16[32,384,1]{1,0,2:T(8,128)(2,1)S(1)}, ...), branch_computations={%region_1.1_spmd, %region_2.5_spmd} | conditional | flops 99241728 | bytes 5755680 | solution.py:77
  414.8 7.2 %conditional.3 = (bf16[1,1,384,128]{3,2,1,0:T(8,128)(2,1)S(1)}, f32[1,1,384]{2,1,0:T(1,128)S(1)}) conditional(s32[]{:T(128)} %convert_element_type.99, () %tuple.52, (s32[]{:T(128)}, s32[]{:T(128)}, bf16[32,384,1,128]{3,1,2,0:T(8,128)(2,1)}, s32[]{:T(128)}, bf16[384,1,128]{2,0,1:T(8,128)(2,1)S(1)}, /*index=5*/bf16[32,384,1]{1,0,2:T(8,128)(2,1)S(1)}, ...), branch_computations={%region_1.1_spmd, %region_2.5_spmd} | conditional | flops 99241728 | bytes 5755680 | solution.py:77
  433.0 7.2 %conditional.3 = (bf16[1,1,384,128]{3,2,1,0:T(8,128)(2,1)S(1)}, f32[1,1,384]{2,1,0:T(1,128)S(1)}) conditional(s32[]{:T(128)} %convert_element_type.99, () %tuple.52, (s32[]{:T(128)}, s32[]{:T(128)}, bf16[32,384,1,128]{3,1,2,0:T(8,128)(2,1)}, s32[]{:T(128)}, bf16[384,1,128]{2,0,1:T(8,128)(2,1)S(1)}, /*index=5*/bf16[32,384,1]{1,0,2:T(8,128)(2,1)S(1)}, ...), branch_computations={%region_1.1_spmd, %region_2.5_spmd} | conditional | flops 99241728 | bytes 5755680 | solution.py:77
  451.2 7.2 %conditional.3 = (bf16[1,1,384,128]{3,2,1,0:T(8,128)(2,1)S(1)}, f32[1,1,384]{2,1,0:T(1,128)S(1)}) conditional(s32[]{:T(128)} %convert_element_type.99, () %tuple.52, (s32[]{:T(128)}, s32[]{:T(128)}, bf16[32,384,1,128]{3,1,2,0:T(8,128)(2,1)}, s32[]{:T(128)}, bf16[384,1,128]{2,0,1:T(8,128)(2,1)S(1)}, /*index=5*/bf16[32,384,1]{1,0,2:T(8,128)(2,1)S(1)}, ...), branch_computations={%region_1.1_spmd, %region_2.5_spmd} | conditional | flops 99241728 | bytes 5755680 | solution.py:77
  460.4 7.2 %conditional.3 = (bf16[1,1,384,128]{3,2,1,0:T(8,128)(2,1)S(1)}, f32[1,1,384]{2,1,0:T(1,128)S(1)}) conditional(s32[]{:T(128)} %convert_element_type.99, () %tuple.52, (s32[]{:T(128)}, s32[]{:T(128)}, bf16[32,384,1,128]{3,1,2,0:T(8,128)(2,1)}, s32[]{:T(128)}, bf16[384,1,128]{2,0,1:T(8,128)(2,1)S(1)}, /*index=5*/bf16[32,384,1]{1,0,2:T(8,128)(2,1)S(1)}, ...), branch_computations={%region_1.1_spmd, %region_2.5_spmd} | conditional | flops 99241728 | bytes 5755680 | solution.py:77
  469.5 7.2 %conditional.3 = (bf16[1,1,384,128]{3,2,1,0:T(8,128)(2,1)S(1)}, f32[1,1,384]{2,1,0:T(1,128)S(1)}) conditional(s32[]{:T(128)} %convert_element_type.99, () %tuple.52, (s32[]{:T(128)}, s32[]{:T(128)}, bf16[32,384,1,128]{3,1,2,0:T(8,128)(2,1)}, s32[]{:T(128)}, bf16[384,1,128]{2,0,1:T(8,128)(2,1)S(1)}, /*index=5*/bf16[32,384,1]{1,0,2:T(8,128)(2,1)S(1)}, ...), branch_computations={%region_1.1_spmd, %region_2.5_spmd} | conditional | flops 99241728 | bytes 5755680 | solution.py:77
  478.6 7.2 %conditional.3 = (bf16[1,1,384,128]{3,2,1,0:T(8,128)(2,1)S(1)}, f32[1,1,384]{2,1,0:T(1,128)S(1)}) conditional(s32[]{:T(128)} %convert_element_type.99, () %tuple.52, (s32[]{:T(128)}, s32[]{:T(128)}, bf16[32,384,1,128]{3,1,2,0:T(8,128)(2,1)}, s32[]{:T(128)}, bf16[384,1,128]{2,0,1:T(8,128)(2,1)S(1)}, /*index=5*/bf16[32,384,1]{1,0,2:T(8,128)(2,1)S(1)}, ...), branch_computations={%region_1.1_spmd, %region_2.5_spmd} | conditional | flops 99241728 | bytes 5755680 | solution.py:77
  487.7 7.2 %conditional.3 = (bf16[1,1,384,128]{3,2,1,0:T(8,128)(2,1)S(1)}, f32[1,1,384]{2,1,0:T(1,128)S(1)}) conditional(s32[]{:T(128)} %convert_element_type.99, () %tuple.52, (s32[]{:T(128)}, s32[]{:T(128)}, bf16[32,384,1,128]{3,1,2,0:T(8,128)(2,1)}, s32[]{:T(128)}, bf16[384,1,128]{2,0,1:T(8,128)(2,1)S(1)}, /*index=5*/bf16[32,384,1]{1,0,2:T(8,128)(2,1)S(1)}, ...), branch_computations={%region_1.1_spmd, %region_2.5_spmd} | conditional | flops 99241728 | bytes 5755680 | solution.py:77
  (557 shorter events, 412.2 us)
Async XLA Ops:
  7.2 68.2 %copy-start = (bf16[1,224,2048]{2,1,0:T(8,128)(2,1)S(1)}, bf16[1,224,2048]{2,1,0:T(8,128)(2,1)}, u32[]{:S(2)}) copy-start(bf16[1,224,2048]{2,1,0:T(8,128)(2,1)} %param.23) | copy-start | bytes 2752516
  7.2 196.4 %all-gather.3.cloned.1.call-start = ((), (), s32[]{:S(2)}) async-start(), calls=%async_computation.4 | async-start | bytes 3244032 | tf_op jit(solution)/shard_map/all_gather | solution.py:44
  17.3 55.3 %all-to-all-start = ((bf16[32,1,16,2048]{3,2,1,0:T(8,128)(2,1)}), bf16[32,1,16,2048]{3,2,1,0:T(8,128)(2,1)S(1)}, u32[]{:S(2)}, u32[]{:S(2)}) async-start(bf16[32,1,16,2048]{3,2,1,0:T(8,128)(2,1)} %bitcast.23), calls=%async_computation | async-start | bytes 4194304 | tf_op jit(solution)/shard_map/all_to_all | solution.py:121
  23.9 179.8 %all-gather.5.cloned.1.call-start = ((), (), s32[]{:S(2)}) async-start(), calls=%async_computation.5 | async-start | bytes 3244032 | tf_op jit(solution)/shard_map/all_gather | solution.py:45
  72.6 2.0 copy-start.3
  135.1 13.1 %copy-start.1 = (bf16[384,1]{0,1:T(2,128)(2,1)S(1)}, bf16[384,1]{0,1:T(2,128)(2,1)}, u32[]{:S(2)}) copy-start(bf16[384,1]{0,1:T(2,128)(2,1)} %param.18) | copy-start | bytes 2308
  135.1 50.4 %copy-start.2 = (f32[128,2]{0,1:T(2,128)S(1)}, f32[128,2]{0,1:T(2,128)}, u32[]{:S(2)}) copy-start(f32[128,2]{0,1:T(2,128)} %param.25) | copy-start | bytes 3076
  138.3 47.3 %all-to-all-start.2 = ((bf16[32,2,1024]{2,1,0:T(2,128)(2,1)}), bf16[32,2,1024]{2,1,0:T(2,128)(2,1)S(1)}, u32[]{:S(2)}, u32[]{:S(2)}) async-start(bf16[32,2,1024]{2,1,0:T(2,128)(2,1)} %reshape.303), calls=%async_computation.2 | async-start | bytes 262144 | tf_op jit(solution)/shard_map/all_to_all | solution.py:132
  187.4 16.2 %copy-start.4 = (bf16[384,128]{1,0:T(8,128)(2,1)S(1)}, bf16[384,128]{1,0:T(8,128)(2,1)}, u32[]{:S(2)}) copy-start(bf16[384,128]{1,0:T(8,128)(2,1)} %param.15) | copy-start | bytes 294916
  187.4 313.0 %all-to-all-start.3 = ((bf16[16,1,32,1,2048]{4,2,3,1,0:T(8,128)(2,1)}), bf16[16,1,32,1,2048]{4,2,3,1,0:T(8,128)(2,1)}, u32[]{:S(2)}, u32[]{:S(2)}) async-start(bf16[16,1,32,1,2048]{4,2,3,1,0:T(8,128)(2,1)} %broadcast_in_dim.46), calls=%async_computation.3 | async-start | bytes 4194304 | tf_op jit(solution)/shard_map/all_to_all | solution.py:28
Sparse Core Ops, SparseCore 0:
  11.1 85.3 all-gather.2
  99.7 81.6 all-gather.4
where the time goes:
time: 522 us; the launch traced here: 519 us
  other arithmetic  151 us (29%)
  blocking collectives  96.1 us (18%)
  matrix products  92.5 us (18%)
  local copies, waits for them, and re-layouts  59.5 us (11%)
  waiting for transfers between devices  49.4 us (9%)
  starting transfers between devices  32.6 us (6%)
  loops' own time  23.3 us (4%)
  between operations  14.3 us (3%)
    another operation x66, other arithmetic  113 us
    all_to_all x1, blocking collectives, sent_and_summed(): lax.all_to_all(parts, axis, split_axis=0, concat_axis=0, tiled=True)  58.9 us
    all_to_all x1, waiting for transfers between devices, routed_experts(): lax.all_to_all(outgoing, 'ep', split_axis=0, concat_axis=0, tiled=True)  48 us
    dot_general x32, matrix products, compute_block(): jnp.einsum('qhd,khd->hqk', query_heads, key_here, preferred_element_type=...  47.9 us
    dot_general x32, matrix products, compute_block(): jnp.einsum('hqk,khd->hqd', local, value_here, preferred_element_type=jnp....  37.3 us
    all_gather x1, blocking collectives, stick_mixer(): offset_piece = lax.all_gather(key_offset, 'ep', axis=0, tiled=True)  37.1 us
    convert_element_type x32, other arithmetic, compute_block(): jnp.where(strict, jnp.exp(jax.nn.log_sigmoid(logits) + within), 0.0)  27.7 us
    another operation x1, loops' own time, stick_mixer(): lax.map(one_block, (key_split, value_split, offset_split, jnp.arange(bloc...  21.2 us
  transfers between devices with their start and end apart: 5, of which 1 were waited for; matrix products, arithmetic and copies ran while one was open for 56% of the time, Pallas kernels for 0%

commit v1 on v0

--- a/solution.py
+++ b/solution.py
@@ -43,7 +43,9 @@
     last_row = (position + 1) * query_len
     key_piece = lax.all_gather(keys, "ep", axis=0, tiled=True)
     value_piece = lax.all_gather(values, "ep", axis=0, tiled=True)
-    offset_piece = lax.all_gather(key_offset, "ep", axis=0, tiled=True)
+    offset_piece = jnp.concatenate(
+        lax.all_to_all(jnp.stack([key_offset] * lax.axis_size("ep")), "ep", 0, 0), axis=0
+    )
     block_count = key_piece.shape[0] // query_len
     key_split = key_piece.reshape(block_count, query_len, heads, head_dim)
     value_split = value_piece.reshape(block_count, query_len, heads, head_dim)

time: 522 us -> 505 us (0.967)
  the two profiles are of different devices: /device:TPU:463 before, /device:TPU:486 now
where the time goes in v1:
time: 505 us; the launch traced here: 502 us
  other arithmetic  152 us (30%)
  waiting for transfers between devices  118 us (23%)
  matrix products  93.9 us (19%)
  local copies, waits for them, and re-layouts  60.4 us (12%)
  starting transfers between devices  40.1 us (8%)
  loops' own time  23.3 us (5%)
  between operations  14.3 us (3%)
    another operation x66, other arithmetic  113 us
    all_to_all x1, waiting for transfers between devices, routed_experts(): lax.all_to_all(outgoing, 'ep', split_axis=0, concat_axis=0, tiled=True)  50.5 us
    dot_general x32, matrix products, compute_block(): jnp.einsum('qhd,khd->hqk', query_heads, key_here, preferred_element_type=...  47.9 us
    all_to_all x1, waiting for transfers between devices, sent_and_summed(): lax.all_to_all(parts, axis, split_axis=0, concat_axis=0, tiled=True)  44.6 us
    dot_general x32, matrix products, compute_block(): jnp.einsum('hqk,khd->hqd', local, value_here, preferred_element_type=jnp....  37.3 us
    convert_element_type x32, other arithmetic, compute_block(): jnp.where(strict, jnp.exp(jax.nn.log_sigmoid(logits) + within), 0.0)  27.7 us
    another operation x1, loops' own time, stick_mixer(): lax.map(one_block, (key_split, value_split, offset_split, jnp.arange(bloc...  21.2 us
    dynamic_update_slice x64, local copies, waits for them, and re-layouts, stick_mixer(): lax.map(one_block, (key_split, value_split, offset_split, jnp.arange(bloc...  21 us
  transfers between devices with their start and end apart: 7, of which 5 were waited for; matrix products, arithmetic and copies ran while one was open for 59% of the time, Pallas kernels for 0%

profile of v1, /device:TPU:486, one launch (start us, length us, event | category | flops | bytes accessed | tf_op | source)
XLA Modules:
  0.0 501.8 jit_solution(5852398344939566793)
XLA Ops:
  25.2 50.5 %all-to-all-done.1 = bf16[32,1,16,2048]{3,2,1,0:T(8,128)(2,1)S(1)} async-done(((bf16[32,1,16,2048]{3,2,1,0:T(8,128)(2,1)}), bf16[32,1,16,2048]{3,2,1,0:T(8,128)(2,1)S(1)}, u32[]{:S(2)}, u32[]{:S(2)}) %all-to-all-start.1) | async-done | bytes 2097184 | tf_op jit(solution)/shard_map/all_to_all | solution.py:123
  80.5 7.4 %all-to-all-start.2 = ((bf16[16,1,32,1,2048]{4,2,3,1,0:T(8,128)(2,1)}), bf16[16,1,32,1,2048]{4,2,3,1,0:T(8,128)(2,1)S(1)}, u32[]{:S(2)}, u32[]{:S(2)}) async-start(bf16[16,1,32,1,2048]{4,2,3,1,0:T(8,128)(2,1)} %fusion.22), calls=%async_computation.2 | async-start | bytes 4194304 | tf_op jit(solution)/shard_map/all_to_all | solution.py:16
  89.9 44.6 %all-to-all-done.2 = bf16[16,1,32,1,2048]{4,2,3,1,0:T(8,128)(2,1)S(1)} async-done(((bf16[16,1,32,1,2048]{4,2,3,1,0:T(8,128)(2,1)}), bf16[16,1,32,1,2048]{4,2,3,1,0:T(8,128)(2,1)S(1)}, u32[]{:S(2)}, u32[]{:S(2)}) %all-to-all-start.2) | async-done | bytes 2097184 | tf_op jit(solution)/shard_map/all_to_all | solution.py:16
  134.5 10.4 %all-to-all-start = ((bf16[32,2,192]{2,1,0:T(2,128)(2,1)}), bf16[32,2,192]{2,1,0:T(2,128)(2,1)S(1)}, u32[]{:S(2)}, u32[]{:S(2)}) async-start(bf16[32,2,192]{2,1,0:T(2,128)(2,1)} %reshape.302), calls=%async_computation | async-start | bytes 65536 | tf_op jit(solution)/shard_map/all_to_all | solution.py:47
  150.7 7.8 %all-to-all-start.3 = ((bf16[32,2,1024]{2,1,0:T(2,128)(2,1)}), bf16[32,2,1024]{2,1,0:T(2,128)(2,1)S(1)}, u32[]{:S(2)}, u32[]{:S(2)}) async-start(bf16[32,2,1024]{2,1,0:T(2,128)(2,1)} %reshape.304), calls=%async_computation.3 | async-start | bytes 262144 | tf_op jit(solution)/shard_map/all_to_all | solution.py:134
  158.9 7.4 %all-to-all-done.3 = bf16[32,2,1024]{2,1,0:T(2,128)(2,1)S(1)} async-done(((bf16[32,2,1024]{2,1,0:T(2,128)(2,1)}), bf16[32,2,1024]{2,1,0:T(2,128)(2,1)S(1)}, u32[]{:S(2)}, u32[]{:S(2)}) %all-to-all-start.3) | async-done | bytes 131104 | tf_op jit(solution)/shard_map/all_to_all | solution.py:134
  168.1 7.4 %all-to-all-start.4 = ((bf16[16,1,32,1,2048]{4,2,3,1,0:T(8,128)(2,1)}), bf16[16,1,32,1,2048]{4,2,3,1,0:T(8,128)(2,1)}, u32[]{:S(2)}, u32[]{:S(2)}) async-start(bf16[16,1,32,1,2048]{4,2,3,1,0:T(8,128)(2,1)} %broadcast_in_dim.46), calls=%async_computation.4 | async-start | bytes 4194304 | tf_op jit(solution)/shard_map/all_to_all | solution.py:28
  175.5 10.9 %all-gather.5.cloned.1.call-done = bf16[12288,128]{1,0:T(8,128)(2,1)} async-done(((bf16[384,128]{1,0:T(8,128)(2,1)}), bf16[12288,128]{1,0:T(8,128)(2,1)}) %all-gather.5.cloned.1.call-update) | async-done | bytes 3145744 | tf_op jit(solution)/shard_map/all_gather | solution.py:45
  186.4 291.9 %while.13 = (s32[]{:T(128)}, bf16[32,1,384,128]{3,2,1,0:T(8,128)(2,1)}, f32[32,1,384]{2,1,0:T(1,128)S(1)}, s32[32]{0:T(128)S(1)}, s32[]{:T(128)}, /*index=5*/bf1...) while((s32[]{:T(128)}, ...), condition=%wide.region_6.7_spmd.clone, body=%wide.region_0.6_spmd.clone.sunk | while | flops 99241728 | bytes 5957639 | solution.py:89
  187.7 7.2 %conditional.3 = (bf16[1,1,384,128]{3,2,1,0:T(8,128)(2,1)S(1)}, f32[1,1,384]{2,1,0:T(1,128)S(1)}) conditional(s32[]{:T(128)} %convert_element_type.99, () %tuple.52, (s32[]{:T(128)}, s32[]{:T(128)}, bf16[32,384,1,128]{3,1,2,0:T(8,128)(2,1)}, s32[]{:T(128)}, bf16[384,1,128]{2,0,1:T(8,128)(2,1)S(1)}, /*index=5*/bf16[32,384,1]{1,0,2:T(8,128)(2,1)S(1)}, ...), branch_computations={%region_1.1_spmd, %region_2.5_spmd} | conditional | flops 99241728 | bytes 5755680 | solution.py:79
  251.6 7.2 %conditional.3 = (bf16[1,1,384,128]{3,2,1,0:T(8,128)(2,1)S(1)}, f32[1,1,384]{2,1,0:T(1,128)S(1)}) conditional(s32[]{:T(128)} %convert_element_type.99, () %tuple.52, (s32[]{:T(128)}, s32[]{:T(128)}, bf16[32,384,1,128]{3,1,2,0:T(8,128)(2,1)}, s32[]{:T(128)}, bf16[384,1,128]{2,0,1:T(8,128)(2,1)S(1)}, /*index=5*/bf16[32,384,1]{1,0,2:T(8,128)(2,1)S(1)}, ...), branch_computations={%region_1.1_spmd, %region_2.5_spmd} | conditional | flops 99241728 | bytes 5755680 | solution.py:79
  260.7 7.2 %conditional.3 = (bf16[1,1,384,128]{3,2,1,0:T(8,128)(2,1)S(1)}, f32[1,1,384]{2,1,0:T(1,128)S(1)}) conditional(s32[]{:T(128)} %convert_element_type.99, () %tuple.52, (s32[]{:T(128)}, s32[]{:T(128)}, bf16[32,384,1,128]{3,1,2,0:T(8,128)(2,1)}, s32[]{:T(128)}, bf16[384,1,128]{2,0,1:T(8,128)(2,1)S(1)}, /*index=5*/bf16[32,384,1]{1,0,2:T(8,128)(2,1)S(1)}, ...), branch_computations={%region_1.1_spmd, %region_2.5_spmd} | conditional | flops 99241728 | bytes 5755680 | solution.py:79
  269.8 7.2 %conditional.3 = (bf16[1,1,384,128]{3,2,1,0:T(8,128)(2,1)S(1)}, f32[1,1,384]{2,1,0:T(1,128)S(1)}) conditional(s32[]{:T(128)} %convert_element_type.99, () %tuple.52, (s32[]{:T(128)}, s32[]{:T(128)}, bf16[32,384,1,128]{3,1,2,0:T(8,128)(2,1)}, s32[]{:T(128)}, bf16[384,1,128]{2,0,1:T(8,128)(2,1)S(1)}, /*index=5*/bf16[32,384,1]{1,0,2:T(8,128)(2,1)S(1)}, ...), branch_computations={%region_1.1_spmd, %region_2.5_spmd} | conditional | flops 99241728 | bytes 5755680 | solution.py:79
  278.9 7.2 %conditional.3 = (bf16[1,1,384,128]{3,2,1,0:T(8,128)(2,1)S(1)}, f32[1,1,384]{2,1,0:T(1,128)S(1)}) conditional(s32[]{:T(128)} %convert_element_type.99, () %tuple.52, (s32[]{:T(128)}, s32[]{:T(128)}, bf16[32,384,1,128]{3,1,2,0:T(8,128)(2,1)}, s32[]{:T(128)}, bf16[384,1,128]{2,0,1:T(8,128)(2,1)S(1)}, /*index=5*/bf16[32,384,1]{1,0,2:T(8,128)(2,1)S(1)}, ...), branch_computations={%region_1.1_spmd, %region_2.5_spmd} | conditional | flops 99241728 | bytes 5755680 | solution.py:79
  288.0 7.2 %conditional.3 = (bf16[1,1,384,128]{3,2,1,0:T(8,128)(2,1)S(1)}, f32[1,1,384]{2,1,0:T(1,128)S(1)}) conditional(s32[]{:T(128)} %convert_element_type.99, () %tuple.52, (s32[]{:T(128)}, s32[]{:T(128)}, bf16[32,384,1,128]{3,1,2,0:T(8,128)(2,1)}, s32[]{:T(128)}, bf16[384,1,128]{2,0,1:T(8,128)(2,1)S(1)}, /*index=5*/bf16[32,384,1]{1,0,2:T(8,128)(2,1)S(1)}, ...), branch_computations={%region_1.1_spmd, %region_2.5_spmd} | conditional | flops 99241728 | bytes 5755680 | solution.py:79
  379.2 7.2 %conditional.3 = (bf16[1,1,384,128]{3,2,1,0:T(8,128)(2,1)S(1)}, f32[1,1,384]{2,1,0:T(1,128)S(1)}) conditional(s32[]{:T(128)} %convert_element_type.99, () %tuple.52, (s32[]{:T(128)}, s32[]{:T(128)}, bf16[32,384,1,128]{3,1,2,0:T(8,128)(2,1)}, s32[]{:T(128)}, bf16[384,1,128]{2,0,1:T(8,128)(2,1)S(1)}, /*index=5*/bf16[32,384,1]{1,0,2:T(8,128)(2,1)S(1)}, ...), branch_computations={%region_1.1_spmd, %region_2.5_spmd} | conditional | flops 99241728 | bytes 5755680 | solution.py:79
  388.4 7.2 %conditional.3 = (bf16[1,1,384,128]{3,2,1,0:T(8,128)(2,1)S(1)}, f32[1,1,384]{2,1,0:T(1,128)S(1)}) conditional(s32[]{:T(128)} %convert_element_type.99, () %tuple.52, (s32[]{:T(128)}, s32[]{:T(128)}, bf16[32,384,1,128]{3,1,2,0:T(8,128)(2,1)}, s32[]{:T(128)}, bf16[384,1,128]{2,0,1:T(8,128)(2,1)S(1)}, /*index=5*/bf16[32,384,1]{1,0,2:T(8,128)(2,1)S(1)}, ...), branch_computations={%region_1.1_spmd, %region_2.5_spmd} | conditional | flops 99241728 | bytes 5755680 | solution.py:79
  397.5 7.2 %conditional.3 = (bf16[1,1,384,128]{3,2,1,0:T(8,128)(2,1)S(1)}, f32[1,1,384]{2,1,0:T(1,128)S(1)}) conditional(s32[]{:T(128)} %convert_element_type.99, () %tuple.52, (s32[]{:T(128)}, s32[]{:T(128)}, bf16[32,384,1,128]{3,1,2,0:T(8,128)(2,1)}, s32[]{:T(128)}, bf16[384,1,128]{2,0,1:T(8,128)(2,1)S(1)}, /*index=5*/bf16[32,384,1]{1,0,2:T(8,128)(2,1)S(1)}, ...), branch_computations={%region_1.1_spmd, %region_2.5_spmd} | conditional | flops 99241728 | bytes 5755680 | solution.py:79
  415.7 7.2 %conditional.3 = (bf16[1,1,384,128]{3,2,1,0:T(8,128)(2,1)S(1)}, f32[1,1,384]{2,1,0:T(1,128)S(1)}) conditional(s32[]{:T(128)} %convert_element_type.99, () %tuple.52, (s32[]{:T(128)}, s32[]{:T(128)}, bf16[32,384,1,128]{3,1,2,0:T(8,128)(2,1)}, s32[]{:T(128)}, bf16[384,1,128]{2,0,1:T(8,128)(2,1)S(1)}, /*index=5*/bf16[32,384,1]{1,0,2:T(8,128)(2,1)S(1)}, ...), branch_computations={%region_1.1_spmd, %region_2.5_spmd} | conditional | flops 99241728 | bytes 5755680 | solution.py:79
  434.0 7.2 %conditional.3 = (bf16[1,1,384,128]{3,2,1,0:T(8,128)(2,1)S(1)}, f32[1,1,384]{2,1,0:T(1,128)S(1)}) conditional(s32[]{:T(128)} %convert_element_type.99, () %tuple.52, (s32[]{:T(128)}, s32[]{:T(128)}, bf16[32,384,1,128]{3,1,2,0:T(8,128)(2,1)}, s32[]{:T(128)}, bf16[384,1,128]{2,0,1:T(8,128)(2,1)S(1)}, /*index=5*/bf16[32,384,1]{1,0,2:T(8,128)(2,1)S(1)}, ...), branch_computations={%region_1.1_spmd, %region_2.5_spmd} | conditional | flops 99241728 | bytes 5755680 | solution.py:79
  443.1 7.2 %conditional.3 = (bf16[1,1,384,128]{3,2,1,0:T(8,128)(2,1)S(1)}, f32[1,1,384]{2,1,0:T(1,128)S(1)}) conditional(s32[]{:T(128)} %convert_element_type.99, () %tuple.52, (s32[]{:T(128)}, s32[]{:T(128)}, bf16[32,384,1,128]{3,1,2,0:T(8,128)(2,1)}, s32[]{:T(128)}, bf16[384,1,128]{2,0,1:T(8,128)(2,1)S(1)}, /*index=5*/bf16[32,384,1]{1,0,2:T(8,128)(2,1)S(1)}, ...), branch_computations={%region_1.1_spmd, %region_2.5_spmd} | conditional | flops 99241728 | bytes 5755680 | solution.py:79
  452.2 7.2 %conditional.3 = (bf16[1,1,384,128]{3,2,1,0:T(8,128)(2,1)S(1)}, f32[1,1,384]{2,1,0:T(1,128)S(1)}) conditional(s32[]{:T(128)} %convert_element_type.99, () %tuple.52, (s32[]{:T(128)}, s32[]{:T(128)}, bf16[32,384,1,128]{3,1,2,0:T(8,128)(2,1)}, s32[]{:T(128)}, bf16[384,1,128]{2,0,1:T(8,128)(2,1)S(1)}, /*index=5*/bf16[32,384,1]{1,0,2:T(8,128)(2,1)S(1)}, ...), branch_computations={%region_1.1_spmd, %region_2.5_spmd} | conditional | flops 99241728 | bytes 5755680 | solution.py:79
  461.4 7.2 %conditional.3 = (bf16[1,1,384,128]{3,2,1,0:T(8,128)(2,1)S(1)}, f32[1,1,384]{2,1,0:T(1,128)S(1)}) conditional(s32[]{:T(128)} %convert_element_type.99, () %tuple.52, (s32[]{:T(128)}, s32[]{:T(128)}, bf16[32,384,1,128]{3,1,2,0:T(8,128)(2,1)}, s32[]{:T(128)}, bf16[384,1,128]{2,0,1:T(8,128)(2,1)S(1)}, /*index=5*/bf16[32,384,1]{1,0,2:T(8,128)(2,1)S(1)}, ...), branch_computations={%region_1.1_spmd, %region_2.5_spmd} | conditional | flops 99241728 | bytes 5755680 | solution.py:79
  470.5 7.2 %conditional.3 = (bf16[1,1,384,128]{3,2,1,0:T(8,128)(2,1)S(1)}, f32[1,1,384]{2,1,0:T(1,128)S(1)}) conditional(s32[]{:T(128)} %convert_element_type.99, () %tuple.52, (s32[]{:T(128)}, s32[]{:T(128)}, bf16[32,384,1,128]{3,1,2,0:T(8,128)(2,1)}, s32[]{:T(128)}, bf16[384,1,128]{2,0,1:T(8,128)(2,1)S(1)}, /*index=5*/bf16[32,384,1]{1,0,2:T(8,128)(2,1)S(1)}, ...), branch_computations={%region_1.1_spmd, %region_2.5_spmd} | conditional | flops 99241728 | bytes 5755680 | solution.py:79
  (563 shorter events, 440.3 us)
Async XLA Ops:
  7.2 71.2 %copy-start = (bf16[1,224,2048]{2,1,0:T(8,128)(2,1)S(1)}, bf16[1,224,2048]{2,1,0:T(8,128)(2,1)}, u32[]{:S(2)}) copy-start(bf16[1,224,2048]{2,1,0:T(8,128)(2,1)} %param.23) | copy-start | bytes 2752516
  7.2 168.3 %all-gather.3.cloned.1.call-start = ((), (), s32[]{:S(2)}) async-start(), calls=%async_computation.5 | async-start | bytes 3244032 | tf_op jit(solution)/shard_map/all_gather | solution.py:44
  17.3 58.4 %all-to-all-start.1 = ((bf16[32,1,16,2048]{3,2,1,0:T(8,128)(2,1)}), bf16[32,1,16,2048]{3,2,1,0:T(8,128)(2,1)S(1)}, u32[]{:S(2)}, u32[]{:S(2)}) async-start(bf16[32,1,16,2048]{3,2,1,0:T(8,128)(2,1)} %bitcast.23), calls=%async_computation.1 | async-start | bytes 4194304 | tf_op jit(solution)/shard_map/all_to_all | solution.py:123
  24.4 162.0 %all-gather.5.cloned.1.call-start = ((), (), s32[]{:S(2)}) async-start(), calls=%async_computation.6 | async-start | bytes 3244032 | tf_op jit(solution)/shard_map/all_gather | solution.py:45
  75.6 2.0 copy-start.3
  80.5 7.4 %copy-start.1 = (bf16[384,1]{0,1:T(2,128)(2,1)S(1)}, bf16[384,1]{0,1:T(2,128)(2,1)}, u32[]{:S(2)}) copy-start(bf16[384,1]{0,1:T(2,128)(2,1)} %param.18) | copy-start | bytes 2308
  80.5 54.0 %all-to-all-start.2 = ((bf16[16,1,32,1,2048]{4,2,3,1,0:T(8,128)(2,1)}), bf16[16,1,32,1,2048]{4,2,3,1,0:T(8,128)(2,1)S(1)}, u32[]{:S(2)}, u32[]{:S(2)}) async-start(bf16[16,1,32,1,2048]{4,2,3,1,0:T(8,128)(2,1)} %fusion.22), calls=%async_computation.2 | async-start | bytes 4194304 | tf_op jit(solution)/shard_map/all_to_all | solution.py:16
  87.8 70.8 %copy-start.2 = (f32[128,2]{0,1:T(2,128)S(1)}, f32[128,2]{0,1:T(2,128)}, u32[]{:S(2)}) copy-start(f32[128,2]{0,1:T(2,128)} %param.25) | copy-start | bytes 3076
  134.5 16.2 %all-to-all-start = ((bf16[32,2,192]{2,1,0:T(2,128)(2,1)}), bf16[32,2,192]{2,1,0:T(2,128)(2,1)S(1)}, u32[]{:S(2)}, u32[]{:S(2)}) async-start(bf16[32,2,192]{2,1,0:T(2,128)(2,1)} %reshape.302), calls=%async_computation | async-start | bytes 65536 | tf_op jit(solution)/shard_map/all_to_all | solution.py:47
  150.7 15.5 %all-to-all-start.3 = ((bf16[32,2,1024]{2,1,0:T(2,128)(2,1)}), bf16[32,2,1024]{2,1,0:T(2,128)(2,1)S(1)}, u32[]{:S(2)}, u32[]{:S(2)}) async-start(bf16[32,2,1024]{2,1,0:T(2,128)(2,1)} %reshape.304), calls=%async_computation.3 | async-start | bytes 262144 | tf_op jit(solution)/shard_map/all_to_all | solution.py:134
  168.1 18.3 %copy-start.4 = (bf16[384,128]{1,0:T(8,128)(2,1)S(1)}, bf16[384,128]{1,0:T(8,128)(2,1)}, u32[]{:S(2)}) copy-start(bf16[384,128]{1,0:T(8,128)(2,1)} %param.15) | copy-start | bytes 294916
  168.1 315.1 %all-to-all-start.4 = ((bf16[16,1,32,1,2048]{4,2,3,1,0:T(8,128)(2,1)}), bf16[16,1,32,1,2048]{4,2,3,1,0:T(8,128)(2,1)}, u32[]{:S(2)}, u32[]{:S(2)}) async-start(bf16[16,1,32,1,2048]{4,2,3,1,0:T(8,128)(2,1)} %broadcast_in_dim.46), calls=%async_computation.4 | async-start | bytes 4194304 | tf_op jit(solution)/shard_map/all_to_all | solution.py:28
Sparse Core Ops, SparseCore 0:
  11.1 88.8 all-gather.2
  103.2 83.1 all-gather.4
